TPU v7x, 32 devices: a whole 2x2x4 slice. The times are simulated.
32 devices in a mesh: sp: 8 (over z, y), tp: 4 (over x, core).
Axes of the slice: x: 2, y: 2, z: 4, core: 2. Of those that a mesh axis runs over, the one named last changes fastest.
Arguments:
- gate_in: bfloat16 [4096, 2048], P('sp', 'tp'), may hold values from -6 to 6
- value_in: bfloat16 [4096, 2048], P('sp', 'tp'), may hold values from -6 to 6
- gate_out: bfloat16 [4096, 2048], P('sp', 'tp'), may hold values from -6 to 6
- conv_taps: float32 [3, 2048], P(None, 'tp'), may hold values from -3.5 to 3.5
- proj_weight: bfloat16 [2048, 2048], P('tp'), may hold values from -0.125 to 0.125
- residual: bfloat16 [4096, 2048], P(('sp', 'tp')), may hold values from -6 to 6
- norm_gain: float32 [2048], replicated, may hold values from 0.1 to 1.9
- routes: int32 [4096, 2], P('sp'), may hold values from 0 to 7, all different within a row; in each aligned block of 128 rows (0 to 127, 128 to 255, ...) at most 64 rows name the same one
- route_weight: float32 [4096, 2], P('sp'), may hold values from 0.1 to 0.9
- expert_gate: bfloat16 [8, 2048, 2048], P('sp', None, 'tp'), may hold values from -0.125 to 0.125
- expert_up: bfloat16 [8, 2048, 2048], P('sp', None, 'tp'), may hold values from -0.125 to 0.125
- expert_down: bfloat16 [8, 2048, 2048], P('sp', 'tp'), may hold values from -0.125 to 0.125
Outputs:
- layer_out: bfloat16 [4096, 2048], P(('sp', 'tp'))
Inputs may be any that keep to these rules, and one draw needn't show every extreme that they name: `routes`: A token's 2 experts differ. In each aligned block of 128 tokens no expert is named by more than 64 tokens, a bound that some block reaches.
All inputs are finite; a program needn't handle non-finite values.
Results may differ from a plain program's by a relative error of at most 0.012.
Values may be sent and summed in bfloat16 or wider, within the bound.
A program may use at most 128 MiB of HBM per device.

v0:
```python
import functools

import jax
import jax.numpy as jnp
from jax import lax
from jax.experimental import pallas as pl
from jax.experimental.pallas import tpu as pltpu
from jax.sharding import PartitionSpec as P


def slot_numbers(route_ids, block_rows, expert_count):
    block_count = route_ids.shape[0] // block_rows
    flat_ids = route_ids.reshape(block_count, block_rows * route_ids.shape[1])
    one_hot = (
        flat_ids[:, :, None] == jnp.arange(expert_count, dtype=jnp.int32)[None, None, :]
    ).astype(jnp.int32)
    before = jnp.cumsum(one_hot, axis=1) - one_hot
    return jnp.sum(before * one_hot, axis=2).reshape(route_ids.shape)


def dispatch_rows(normed, flat_pick, slot_count):
    slot_ids = jnp.arange(slot_count, dtype=jnp.int32)
    chosen = jnp.any(flat_pick[None, :, :] == slot_ids[:, None, None], axis=2)
    return jnp.dot(
        chosen.astype(jnp.bfloat16), normed, preferred_element_type=jnp.float32
    ).astype(jnp.bfloat16)


MESH = pl.DeviceIdType.MESH


def mixer_kernel(
    n, tp, halo, pieces, gate_ref, value_ref, out_gate_ref, taps_ref, proj_ref, res_ref, gain_ref,
    rows_ref, normed_ref, edge, product, mixed, part, mrecv, psum, xrecv, send, got,
):
    s = lax.axis_index("sp")
    t = lax.axis_index("tp")
    mate = t + 1 - 2 * (t % 2)
    across = (t + 2) % tp
    mate_across = (mate + 2) % tp
    tokens = gate_ref.shape[0]
    quarter, width = res_ref.shape
    piece = quarter // pieces
    after, before = (s + 1) % n, (s + n - 1) % n

    barrier = pltpu.get_barrier_semaphore()
    for peer in ((s, mate), (s, across), (after, t), (before, t)):
        pl.semaphore_signal(barrier, inc=1, device_id=peer, device_id_type=MESH)

    def remote(src, dst, lane, device):
        return pltpu.make_async_remote_copy(
            src_ref=src,
            dst_ref=dst,
            send_sem=send.at[lane],
            recv_sem=got.at[lane],
            device_id=device,
            device_id_type=MESH,
        )

    tail = pl.ds(tokens - halo, halo)
    edges = [
        remote(ref.at[tail], edge.at[i], i, (after, t))
        for i, ref in enumerate((gate_ref, value_ref))
    ]
    pl.semaphore_wait(barrier, 4)
    for copy in edges:
        copy.start()

    body_rows = pl.ds(halo, tokens)
    product[body_rows] = gate_ref[...].astype(jnp.float32) * value_ref[...].astype(jnp.float32)
    for copy in edges:
        copy.wait_recv()
    prior = edge[0].astype(jnp.float32) * edge[1].astype(jnp.float32)
    product[pl.ds(0, halo)] = jnp.where(s == 0, 0.0, prior)
    conv_sum = (
        taps_ref[0:1] * product[pl.ds(halo - 2, tokens)]
        + taps_ref[1:2] * product[pl.ds(halo - 1, tokens)]
        + taps_ref[2:3] * product[body_rows]
    )
    mixed[...] = (out_gate_ref[...].astype(jnp.float32) * conv_sum).astype(jnp.bfloat16)

    def project(block, p):
        first = pl.multiple_of(block * quarter + p * piece, piece)
        y = jnp.dot(
            mixed[pl.ds(first, piece)], proj_ref[...], preferred_element_type=jnp.float32
        )
        part[block, p] = y.astype(jnp.bfloat16)

    def lane(kind, p):
        return 2 + kind * pieces + p

    def to_mate(kind, block, p):
        return remote(part.at[block, p], mrecv.at[kind, p], lane(kind, p), (s, mate))

    def over(p):
        return remote(psum.at[p], xrecv.at[p], lane(2, p), (s, across))

    def wide(block):
        return block.astype(jnp.float32)

    for p in range(pieces):
        project(mate_across, p)
        to_mate(0, mate_across, p).start()
    for p in range(pieces):
        project(across, p)
        to_mate(0, mate_across, p).wait_recv()
        psum[p] = (wide(part[across, p]) + wide(mrecv[0, p])).astype(jnp.bfloat16)
        over(p).start()
    for p in range(pieces):
        project(mate, p)
        to_mate(1, mate, p).start()
    for p in range(pieces):
        project(t, p)
    for p in range(pieces):
        to_mate(1, mate, p).wait_recv()
        over(p).wait_recv()
        at = pl.ds(p * piece, piece)
        summed = wide(part[t, p]) + wide(mrecv[1, p]) + wide(xrecv[p])
        hidden_rows = wide(res_ref[at]) + summed
        inverse = lax.rsqrt(jnp.mean(hidden_rows * hidden_rows, axis=-1, keepdims=True) + 1e-05)
        rows_ref[at] = hidden_rows
        normed_ref[at] = (hidden_rows * inverse * gain_ref[...]).astype(jnp.bfloat16)
    for copy in edges:
        copy.wait_send()
    for p in range(pieces):
        to_mate(0, mate_across, p).wait_send()
        to_mate(1, mate, p).wait_send()
        over(p).wait_send()


def run_mixer(gate_in, value_in, gate_out, conv_taps, proj_weight, residual, norm_gain):
    n, tp = lax.axis_size("sp"), lax.axis_size("tp")
    tokens, channels = gate_in.shape
    quarter, width = residual.shape
    halo, pieces = 16, 4
    piece = quarter // pieces
    vmem = pl.BlockSpec(memory_space=pltpu.VMEM)
    bf16, f32 = jnp.bfloat16, jnp.float32
    return pl.pallas_call(
        functools.partial(mixer_kernel, n, tp, halo, pieces),
        out_shape=(
            jax.ShapeDtypeStruct((quarter, width), f32),
            jax.ShapeDtypeStruct((quarter, width), bf16),
        ),
        in_specs=[vmem] * 7,
        out_specs=(vmem, vmem),
        scratch_shapes=[
            pltpu.VMEM((2, halo, channels), bf16),
            pltpu.VMEM((halo + tokens, channels), f32),
            pltpu.VMEM((tokens, channels), bf16),
            pltpu.VMEM((tp, pieces, piece, width), bf16),
            pltpu.VMEM((2, pieces, piece, width), bf16),
            pltpu.VMEM((pieces, piece, width), bf16),
            pltpu.VMEM((pieces, piece, width), bf16),
            pltpu.SemaphoreType.DMA((2 + 3 * pieces,)),
            pltpu.SemaphoreType.DMA((2 + 3 * pieces,)),
        ],
        compiler_params=pltpu.CompilerParams(
            collective_id=2, has_side_effects=True, vmem_limit_bytes=60 * 1024 * 1024
        ),
    )(gate_in, value_in, gate_out, conv_taps, proj_weight, residual, norm_gain.reshape(1, width))


def expert_kernel(
    n, tp, halves, out_ref, gate_hbm, up_hbm, down_hbm, ret_ref,
    recv, part, mrecv, psum, xrecv, fin, gate_w, up_w, down_w, hid, local_sem, send, got,
):
    s = lax.axis_index("sp")
    t = lax.axis_index("tp")
    mate = t + 1 - 2 * (t % 2)
    across = (t + 2) % tp
    mate_across = (mate + 2) % tp
    cap, width = out_ref.shape[1], out_ref.shape[2]
    units = gate_w.shape[1]
    rows = tp * cap
    steps = n * halves

    weight_copies = [
        pltpu.make_async_copy(src, dst, local_sem.at[i])
        for i, (src, dst) in enumerate(
            [(gate_hbm, gate_w), (up_hbm, up_w), (down_hbm, down_w)]
        )
    ]
    for copy in weight_copies:
        copy.start()

    barrier = pltpu.get_barrier_semaphore()

    @pl.loop(1, n)
    def _(k):
        pl.semaphore_signal(barrier, inc=1, device_id=((s + k) % n, t), device_id_type=MESH)

    for peer in (mate, across):
        pl.semaphore_signal(barrier, inc=1, device_id=(s, peer), device_id_type=MESH)
    pl.semaphore_wait(barrier, n + 1)

    def remote(src, dst, lane, k, device):
        return pltpu.make_async_remote_copy(
            src_ref=src,
            dst_ref=dst,
            send_sem=send.at[lane, k],
            recv_sem=got.at[lane, k],
            device_id=device,
            device_id_type=MESH,
        )

    def outward(k):
        to = (s + k // halves) % n
        return remote(out_ref.at[to * halves + k % halves], recv.at[k, t], 0, k, (to, t))

    def over(k, block):
        return remote(recv.at[k, block], recv.at[k, block], 1, k, (s, across))

    def pair_own(k, block):
        return remote(recv.at[k, block], recv.at[k, block], 2, k, (s, mate))

    def pair_far(k, block):
        return remote(recv.at[k, block], recv.at[k, block], 3, k, (s, mate))

    def part_near(k):
        return remote(part.at[k, mate], mrecv.at[k, 0], 4, k, (s, mate))

    def part_far(k):
        return remote(part.at[k, mate_across], mrecv.at[k, 1], 5, k, (s, mate))

    def sum_over(k):
        return remote(psum.at[k], xrecv.at[k], 6, k, (s, across))

    def homeward(k):
        to = (s + n - k // halves) % n
        return remote(fin.at[k], ret_ref.at[s * halves + k % halves], 7, k, (to, t))

    own = [
        pltpu.make_async_copy(out_ref.at[s * halves + h], recv.at[h, t], local_sem.at[3 + h])
        for h in range(halves)
    ]
    for copy in own:
        copy.start()

    @pl.loop(halves, steps)
    def _(k):
        outward(k).start()

    for copy in own:
        copy.wait()

    def ffn(k):
        def load():
            block = recv[k]
            if cap % 16:
                return block.astype(jnp.float32).reshape(rows, width).astype(jnp.bfloat16)
            return block.reshape(rows, width)

        cols = min(256, units)

        @pl.loop(0, units // cols)
        def _(c):
            at = pl.ds(pl.multiple_of(c * cols, cols), cols)
            x = load()
            gate = jnp.dot(x, gate_w[:, at], preferred_element_type=jnp.float32)
            up = jnp.dot(x, up_w[:, at], preferred_element_type=jnp.float32)
            hid[:, at] = (gate / (1.0 + jnp.exp(-gate)) * up).astype(jnp.bfloat16)

        wide = min(512, width)

        @pl.loop(0, width // wide)
        def _(c):
            at = pl.ds(pl.multiple_of(c * wide, wide), wide)
            y = jnp.dot(hid[...], down_w[:, at], preferred_element_type=jnp.float32)
            part[k, :, :, at] = y.reshape(tp, cap, wide).astype(jnp.bfloat16)

    def wide_sum(*blocks):
        total = blocks[0].astype(jnp.float32)
        for block in blocks[1:]:
            total = total + block.astype(jnp.float32)
        return total

    @pl.loop(0, steps + 4)
    def _(i):
        @pl.when(i < steps)
        def _():
            @pl.when(i >= halves)
            def _():
                outward(i).wait_recv()

            over(i, t).start()
            pair_own(i, t).start()

        @pl.when((i >= 1) & (i < steps + 1))
        def _():
            k = i - 1
            over(k, across).wait_recv()
            pair_far(k, across).start()

        @pl.when((i >= 3) & (i < steps + 3))
        def _():
            k = i - 3
            part_far(k).wait_recv()
            psum[k] = wide_sum(part[k, across], mrecv[k, 1]).astype(jnp.bfloat16)
            sum_over(k).start()

        @pl.when(i >= 4)
        def _():
            k = i - 4
            part_near(k).wait_recv()
            sum_over(k).wait_recv()
            total = wide_sum(part[k, t], mrecv[k, 0], xrecv[k]).astype(jnp.bfloat16)

            @pl.when(k < halves)
            def _():
                ret_ref[s * halves + k] = total

            @pl.when(k >= halves)
            def _():
                fin[k] = total
                homeward(k).start()

        @pl.when(i == 2)
        def _():
            for copy in weight_copies:
                copy.wait()

        @pl.when((i >= 2) & (i < steps + 2))
        def _():
            k = i - 2
            pair_own(k, mate).wait_recv()
            pair_far(k, mate_across).wait_recv()
            ffn(k)
            part_far(k).start()
            part_near(k).start()

    @pl.loop(0, steps)
    def _(k):
        over(k, t).wait_send()
        pair_own(k, t).wait_send()
        pair_far(k, across).wait_send()
        part_near(k).wait_send()
        part_far(k).wait_send()
        sum_over(k).wait_send()

        @pl.when(k >= halves)
        def _():
            outward(k).wait_send()
            homeward(k).wait_send()
            homeward(k).wait_recv()


def run_experts(outgoing, gate_weight, up_weight, down_weight):
    n, cap, width = outgoing.shape
    tp = lax.axis_size("tp")
    units = gate_weight.shape[1]
    halves = 2 if cap % 32 == 0 else 1
    steps, cap = n * halves, cap // halves
    vmem = pl.BlockSpec(memory_space=pltpu.VMEM)
    hbm = pl.BlockSpec(memory_space=pl.ANY)
    bf16 = jnp.bfloat16
    return pl.pallas_call(
        functools.partial(expert_kernel, n, tp, halves),
        out_shape=jax.ShapeDtypeStruct((steps, cap, width), bf16),
        in_specs=[vmem, hbm, hbm, hbm],
        out_specs=vmem,
        scratch_shapes=[
            pltpu.VMEM((steps, tp, cap, width), bf16),
            pltpu.VMEM((steps, tp, cap, width), bf16),
            pltpu.VMEM((steps, 2, cap, width), bf16),
            pltpu.VMEM((steps, cap, width), bf16),
            pltpu.VMEM((steps, cap, width), bf16),
            pltpu.VMEM((steps, cap, width), bf16),
            pltpu.VMEM(gate_weight.shape, bf16),
            pltpu.VMEM(up_weight.shape, bf16),
            pltpu.VMEM(down_weight.shape, bf16),
            pltpu.VMEM((tp * cap, units), bf16),
            pltpu.SemaphoreType.DMA((3 + halves,)),
            pltpu.SemaphoreType.DMA((8, steps)),
            pltpu.SemaphoreType.DMA((8, steps)),
        ],
        compiler_params=pltpu.CompilerParams(
            collective_id=1, has_side_effects=True, vmem_limit_bytes=60 * 1024 * 1024
        ),
    )(outgoing.reshape(steps, cap, width), gate_weight, up_weight, down_weight)


def exchange_body(
    gate_in,
    value_in,
    gate_out,
    conv_taps,
    proj_weight,
    residual,
    norm_gain,
    routes,
    route_weight,
    expert_gate,
    expert_up,
    expert_down,
):
    model_width = residual.shape[1]
    tp_count = lax.axis_size("tp")
    groups = lax.axis_size("sp")
    quarter = residual.shape[0]
    top_count = routes.shape[1]
    capacity = 2 * quarter * top_count // groups
    tp_index = lax.axis_index("tp")
    first_own = tp_index * quarter
    own_routes = lax.dynamic_slice_in_dim(routes, first_own, quarter, 0)
    own_weights = lax.dynamic_slice_in_dim(route_weight, first_own, quarter, 0)
    my_rows, normed = run_mixer(
        gate_in, value_in, gate_out, conv_taps, proj_weight, residual, norm_gain
    )
    own_slots = slot_numbers(own_routes, quarter, groups)
    flat_pick = own_routes * capacity + own_slots
    slot_count = groups * capacity
    outgoing = dispatch_rows(normed, flat_pick, slot_count)
    returned = run_experts(
        outgoing.reshape(groups, capacity, model_width),
        expert_gate[0],
        expert_up[0],
        expert_down[0],
    ).reshape(slot_count, model_width)
    total = my_rows
    for k in range(top_count):
        pick = flat_pick[:, k, None] == jnp.arange(slot_count, dtype=jnp.int32)
        picked = jnp.dot(
            pick.astype(jnp.bfloat16), returned, preferred_element_type=jnp.float32
        )
        total = total + own_weights[:, k, None] * picked
    return total.astype(jnp.bfloat16)


def plane_of(j, z, planes):
    upper = z >= planes // 2
    near = jnp.where(upper, planes - 1 - z, z)
    swing = jnp.where(j % 2 == 1, near - (j + 1) // 2, near + j // 2)
    place = jnp.where(j <= 2 * near, swing, j)
    return jnp.where(upper, planes - 1 - place, place)


def layer_kernel(
    n, tp, halo, pieces, cap,
    routes_ref, weights_ref, taps_ref, gain_ref,
    gate_hbm, value_hbm, out_gate_hbm, proj_hbm, res_hbm, wg_hbm, wu_hbm, wd_hbm,
    out_ref,
    gate_ref, value_ref, out_gate_ref, proj_ref, res_ref, gate_w, up_w, down_w,
    edge, product, mixed, mpart, mmate, msum, mfar,
    rows, info, spread, raw, ysend, recv, part, mrecv, psum, xrecv, fin, ret, hid,
    local_sem, msend, mgot, isend, igot, rsend, rgot, ysem, ygot, dsend, dgot, psend, pgot, hsend, hgot,
):
    s = lax.axis_index("sp")
    t = lax.axis_index("tp")
    planes = n // 2
    z, y = s // 2, s % 2
    other_y = 1 - y
    mate = t + 1 - 2 * (t % 2)
    across = (t + 2) % tp
    mate_across = (mate + 2) % tp
    tokens = gate_ref.shape[0]
    quarter, width = res_ref.shape
    piece = quarter // pieces
    half = cap // 2
    units = 2 * planes
    after, before = (s + 1) % n, (s + n - 1) % n
    f32, bf16 = jnp.float32, jnp.bfloat16

    loads = [
        pltpu.make_async_copy(src, dst, local_sem.at[i])
        for i, (src, dst) in enumerate(
            [
                (gate_hbm, gate_ref), (value_hbm, value_ref), (out_gate_hbm, out_gate_ref),
                (proj_hbm, proj_ref), (res_hbm, res_ref),
                (wg_hbm, gate_w), (wu_hbm, up_w), (wd_hbm, down_w),
            ]
        )
    ]
    for copy in loads[:5]:
        copy.start()

    barrier = pltpu.get_barrier_semaphore()

    @pl.loop(1, n)
    def _(k):
        pl.semaphore_signal(barrier, inc=1, device_id=((s + k) % n, t), device_id_type=MESH)

    for peer in (mate, across):
        pl.semaphore_signal(barrier, inc=1, device_id=(s, peer), device_id_type=MESH)

    def remote(src, dst, send_sem, recv_sem, device):
        return pltpu.make_async_remote_copy(
            src_ref=src, dst_ref=dst, send_sem=send_sem, recv_sem=recv_sem,
            device_id=device, device_id_type=MESH,
        )

    own_at = pl.ds(pl.multiple_of(t * quarter, quarter), quarter)
    named = [routes_ref[k:k + 1, own_at] for k in range(2)]
    expert_ids = lax.broadcasted_iota(jnp.int32, (n, quarter), 0)
    one_hot = [(expert_ids == name).astype(f32) for name in named]
    earlier = (
        lax.broadcasted_iota(jnp.int32, (quarter, quarter), 0)
        < lax.broadcasted_iota(jnp.int32, (quarter, quarter), 1)
    ).astype(bf16)
    count = jnp.dot(
        (one_hot[0] + one_hot[1]).astype(bf16), earlier, preferred_element_type=f32
    )
    picks = [
        name.astype(f32) * cap + jnp.sum(count * hot, axis=0, keepdims=True)
        for name, hot in zip(named, one_hot)
    ]
    info[z] = jnp.concatenate(picks + [jnp.zeros((6, quarter), f32)], axis=0)

    for copy in loads[:2]:
        copy.wait()
    tail = pl.ds(tokens - halo, halo)
    edges = [
        remote(ref.at[tail], edge.at[i], msend.at[i], mgot.at[i], (after, t))
        for i, ref in enumerate((gate_ref, value_ref))
    ]
    pl.semaphore_wait(barrier, n + 1)
    for copy in edges:
        copy.start()

    def tell(k):
        to = (z + k) % planes
        return remote(info.at[z], info.at[z], isend.at[k], igot.at[z], (to * 2 + y, t))

    def told(k):
        origin = (z + k) % planes
        return remote(info.at[origin], info.at[origin], isend.at[k], igot.at[origin], (s, mate))

    @pl.loop(1, planes)
    def _(k):
        tell(k).start()

    for copy in loads[5:]:
        copy.start()

    body_rows = pl.ds(halo, tokens)
    product[body_rows] = gate_ref[...].astype(f32) * value_ref[...].astype(f32)
    for copy in edges:
        copy.wait_recv()
    prior = edge[0].astype(f32) * edge[1].astype(f32)
    product[pl.ds(0, halo)] = jnp.where(s == 0, 0.0, prior)
    conv_sum = (
        taps_ref[0:1] * product[pl.ds(halo - 2, tokens)]
        + taps_ref[1:2] * product[pl.ds(halo - 1, tokens)]
        + taps_ref[2:3] * product[body_rows]
    )
    loads[2].wait()
    mixed[...] = (out_gate_ref[...].astype(f32) * conv_sum).astype(bf16)
    loads[3].wait()

    def project(block, p):
        first = pl.multiple_of(block * quarter + p * piece, piece)
        y_block = jnp.dot(mixed[pl.ds(first, piece)], proj_ref[...], preferred_element_type=f32)
        mpart[block, p] = y_block.astype(bf16)

    def lane(kind, p):
        return 2 + kind * pieces + p

    def to_mate(kind, block, p):
        at = lane(kind, p)
        return remote(mpart.at[block, p], mmate.at[kind, p], msend.at[at], mgot.at[at], (s, mate))

    def to_across(p):
        at = lane(2, p)
        return remote(msum.at[p], mfar.at[p], msend.at[at], mgot.at[at], (s, across))

    for p in range(pieces):
        project(mate_across, p)
        to_mate(0, mate_across, p).start()
    for p in range(pieces):
        project(across, p)
        to_mate(0, mate_across, p).wait_recv()
        msum[p] = (mpart[across, p].astype(f32) + mmate[0, p].astype(f32)).astype(bf16)
        to_across(p).start()
    for p in range(pieces):
        project(mate, p)
        to_mate(1, mate, p).start()
    for p in range(pieces):
        project(t, p)

    slot_ids = lax.broadcasted_iota(jnp.int32, (n * cap, quarter), 0).astype(f32)
    share = jnp.where(slot_ids == picks[0], weights_ref[0:1, own_at], 0.0) + jnp.where(
        slot_ids == picks[1], weights_ref[1:2, own_at], 0.0
    )
    share = jnp.transpose(share)
    high = share.astype(bf16)
    spread[0] = high
    spread[1] = (share - high.astype(f32)).astype(bf16)

    loads[4].wait()
    for p in range(pieces):
        to_mate(1, mate, p).wait_recv()
        to_across(p).wait_recv()
        at = pl.ds(p * piece, piece)
        summed = (
            mpart[t, p].astype(f32) + mmate[1, p].astype(f32) + mfar[p].astype(f32)
        )
        hidden_rows = res_ref[at].astype(f32) + summed
        inverse = lax.rsqrt(jnp.mean(hidden_rows * hidden_rows, axis=-1, keepdims=True) + 1e-05)
        rows[at] = hidden_rows
        raw[z, at] = (hidden_rows * inverse * gain_ref[...]).astype(bf16)

    def along(block, up):
        to = jnp.where(up == 1, z + 1, z - 1)
        return remote(raw.at[block], raw.at[block], rsend.at[up, block], rgot.at[block], (to * 2 + y, t))

    def has_up(block):
        return (block <= z) & (z < planes - 1)

    def has_down(block):
        return (block >= z) & (z > 0)

    def pass_on(block):
        @pl.when(has_up(block))
        def _():
            along(block, 1).start()

        @pl.when(has_down(block))
        def _():
            along(block, 0).start()

    def beside(j, h):
        return remote(
            ysend.at[j, h], recv.at[j, h, t, y], ysem.at[j, h], ygot.at[j, h], (z * 2 + other_y, t)
        )

    def over(j, h, source):
        ref = recv.at[j, h, t, source]
        return remote(ref, ref, dsend.at[0, j, h, source], dgot.at[0, j, h, source], (s, across))

    def pair_own(j, h, source):
        ref = recv.at[j, h, t, source]
        return remote(ref, ref, dsend.at[1, j, h, source], dgot.at[1, j, h, source], (s, mate))

    def pair_far(j, h, source):
        ref = recv.at[j, h, across, source]
        return remote(ref, ref, dsend.at[2, j, h, source], dgot.at[2, j, h, source], (s, mate))

    wide = min(512, width)

    def select(j, block, expert, put):
        place = lax.broadcasted_iota(jnp.int32, (cap, quarter), 0).astype(f32) + (
            expert * cap
        ).astype(f32)
        table = info[block]
        chosen = ((place == table[0:1]) | (place == table[1:2])).astype(f32).astype(bf16)

        @pl.loop(0, width // wide)
        def _(c):
            at = pl.ds(pl.multiple_of(c * wide, wide), wide)
            taken = jnp.dot(chosen, raw[block, :, at], preferred_element_type=f32).astype(bf16)
            for h in range(2):
                put(h, at, taken[h * half:(h + 1) * half])

    def dispatch(j):
        block = plane_of(j, z, planes)

        @pl.when(j > 0)
        def _():
            along(block, 1).wait_recv()

        pass_on(block)

        @pl.when(j > 0)
        def _():
            told((block + planes - z) % planes).wait_recv()

        def put_own(h, at, value):
            recv[j, h, t, y, :, at] = value

        def put_other(h, at, value):
            ysend[j, h, :, at] = value

        select(j, block, s, put_own)
        for h in (1, 0):
            over(j, h, y).start()
        select(j, block, z * 2 + other_y, put_other)
        for h in (1, 0):
            beside(j, h).start()
        for h in (1, 0):
            pair_own(j, h, y).start()

    def dispatch_beside(j):
        for h in (1, 0):
            beside(j, h).wait_recv()
            over(j, h, other_y).start()
            pair_own(j, h, other_y).start()

    def dispatch_far(j):
        for source in (y, other_y):
            for h in (1, 0):
                over(j, h, source).wait_recv()
                pair_far(j, h, source).start()

    def group(u):
        return (u + 1) // 2 % planes, (u + 1) % 2

    def part_near(u):
        return remote(part.at[u, mate], mrecv.at[u, 0], psend.at[0, u], pgot.at[0, u], (s, mate))

    def part_far(u):
        return remote(part.at[u, mate_across], mrecv.at[u, 1], psend.at[1, u], pgot.at[1, u], (s, mate))

    def sum_over(u):
        return remote(psum.at[u], xrecv.at[u], psend.at[2, u], pgot.at[2, u], (s, across))

    def ffn(u):
        j, h = group(u)
        for source in range(2):
            pair_own(j, h, source).wait_recv()
            pair_far(j, h, source).wait_recv()
        count = gate_w.shape[1]
        cols = min(256, count)

        @pl.loop(0, count // cols)
        def _(c):
            at = pl.ds(pl.multiple_of(c * cols, cols), cols)
            x = recv[j, h].reshape(tp * cap, width)
            gate = jnp.dot(x, gate_w[:, at], preferred_element_type=f32)
            up = jnp.dot(x, up_w[:, at], preferred_element_type=f32)
            hid[:, at] = (gate / (1.0 + jnp.exp(-gate)) * up).astype(bf16)

        @pl.loop(0, width // wide)
        def _(c):
            at = pl.ds(pl.multiple_of(c * wide, wide), wide)
            out = jnp.dot(hid[...], down_w[:, at], preferred_element_type=f32)
            part[u, :, :, :, at] = out.reshape(tp, 2, half, wide).astype(bf16)

        part_far(u).start()
        part_near(u).start()

    def homeward(u, source):
        j, h = group(u)
        to = plane_of(j, z, planes) * 2 + source
        return remote(fin.at[u, source], ret.at[s, h], hsend.at[u, source], hgot.at[s, h], (to, t))

    def returned(origin, h):
        return remote(ret.at[origin, h], ret.at[origin, h], hsend.at[0, 0], hgot.at[origin, h], (s, mate))

    def sum_far(u):
        part_far(u).wait_recv()
        psum[u] = (part[u, across].astype(f32) + mrecv[u, 1].astype(f32)).astype(bf16)
        sum_over(u).start()

    def send_home(u):
        j, h = group(u)
        part_near(u).wait_recv()
        sum_over(u).wait_recv()
        total = (
            part[u, t].astype(f32) + mrecv[u, 0].astype(f32) + xrecv[u].astype(f32)
        ).astype(bf16)
        fin[u] = total

        @pl.when(j == 0)
        def _():
            ret[s, h] = fin[u, y]
            homeward(u, other_y).start()

        @pl.when(j > 0)
        def _():
            for source in range(2):
                homeward(u, source).start()

    dispatch(0)
    dispatch_beside(0)
    for copy in loads[5:]:
        copy.wait()

    @pl.loop(0, planes + 1)
    def _(j):
        @pl.when(j + 1 < planes)
        def _():
            dispatch(j + 1)

        @pl.when(j < planes)
        def _():
            dispatch_far(j)

        first = 2 * j - 1

        @pl.when(j > 0)
        def _():
            ffn(first)

        @pl.when(j + 1 < planes)
        def _():
            dispatch_beside(j + 1)

        @pl.when(j < planes)
        def _():
            ffn(2 * j)

        @pl.when(j > 0)
        def _():
            sum_far(first)

        @pl.when(j > 1)
        def _():
            send_home(first - 2)

        @pl.when(j > 0)
        def _():
            send_home(first - 1)

        @pl.when(j < planes)
        def _():
            sum_far(2 * j)

    send_home(units - 1)

    def gather(plane, put):
        for source in range(2):
            for h in range(2):
                origin = plane * 2 + source

                @pl.when(origin != s)
                def _():
                    returned(origin, h).wait_recv()

        slots = pl.ds(pl.multiple_of(plane * 2 * cap, 2 * cap), 2 * cap)

        @pl.loop(0, width // wide)
        def _(c):
            at = pl.ds(pl.multiple_of(c * wide, wide), wide)
            got = ret[pl.ds(plane * 2, 2), :, :, at].reshape(2 * cap, wide)
            put(
                at,
                rows[:, at]
                + jnp.dot(spread[0, :, slots], got, preferred_element_type=f32)
                + jnp.dot(spread[1, :, slots], got, preferred_element_type=f32),
            )

    def keep(at, value):
        rows[:, at] = value

    def finish(at, value):
        out_ref[:, at] = value.astype(bf16)

    @pl.loop(1, planes)
    def _(j):
        gather(plane_of(j, z, planes), keep)

    gather(z, finish)

    for copy in edges:
        copy.wait_send()
    for p in range(pieces):
        to_mate(0, mate_across, p).wait_send()
        to_mate(1, mate, p).wait_send()
        to_across(p).wait_send()

    @pl.loop(0, planes)
    def _(j):
        @pl.when(j > 0)
        def _():
            tell(j).wait_send()

        @pl.when(has_up(j))
        def _():
            along(j, 1).wait_send()

        @pl.when(has_down(j))
        def _():
            along(j, 0).wait_send()

        for h in range(2):
            beside(j, h).wait_send()
            for source in range(2):
                over(j, h, source).wait_send()
                pair_own(j, h, source).wait_send()
                pair_far(j, h, source).wait_send()

    @pl.loop(0, units)
    def _(u):
        part_near(u).wait_send()
        part_far(u).wait_send()
        sum_over(u).wait_send()
        j, h = group(u)
        homeward(u, other_y).wait_send()

        @pl.when(j > 0)
        def _():
            homeward(u, y).wait_send()


def relay_body(
    gate_in, value_in, gate_out, conv_taps, proj_weight, residual, norm_gain,
    routes, route_weight, expert_gate, expert_up, expert_down,
):
    n, tp = lax.axis_size("sp"), lax.axis_size("tp")
    tokens, channels = gate_in.shape
    quarter, width = residual.shape
    cap = 2 * quarter * routes.shape[1] // n
    units_hidden = expert_gate.shape[2]
    planes, half = n // 2, cap // 2
    units = 2 * planes
    halo, pieces = 16, 4
    piece = quarter // pieces
    vmem = pl.BlockSpec(memory_space=pltpu.VMEM)
    hbm = pl.BlockSpec(memory_space=pl.ANY)
    bf16, f32 = jnp.bfloat16, jnp.float32
    dma = pltpu.SemaphoreType.DMA
    rows = (2, half, width)
    return pl.pallas_call(
        functools.partial(layer_kernel, n, tp, halo, pieces, cap),
        out_shape=jax.ShapeDtypeStruct((quarter, width), bf16),
        in_specs=[vmem] * 4 + [hbm] * 8,
        out_specs=vmem,
        scratch_shapes=[
            pltpu.VMEM((tokens, channels), bf16),
            pltpu.VMEM((tokens, channels), bf16),
            pltpu.VMEM((tokens, channels), bf16),
            pltpu.VMEM(proj_weight.shape, bf16),
            pltpu.VMEM((quarter, width), bf16),
            pltpu.VMEM((width, units_hidden), bf16),
            pltpu.VMEM((width, units_hidden), bf16),
            pltpu.VMEM((units_hidden, width), bf16),
            pltpu.VMEM((2, halo, channels), bf16),
            pltpu.VMEM((halo + tokens, channels), f32),
            pltpu.VMEM((tokens, channels), bf16),
            pltpu.VMEM((tp, pieces, piece, width), bf16),
            pltpu.VMEM((2, pieces, piece, width), bf16),
            pltpu.VMEM((pieces, piece, width), bf16),
            pltpu.VMEM((pieces, piece, width), bf16),
            pltpu.VMEM((quarter, width), f32),
            pltpu.VMEM((planes, 8, quarter), f32),
            pltpu.VMEM((2, quarter, n * cap), bf16),
            pltpu.VMEM((planes, quarter, width), bf16),
            pltpu.VMEM((planes,) + rows, bf16),
            pltpu.VMEM((planes, 2, tp) + rows, bf16),
            pltpu.VMEM((units, tp) + rows, bf16),
            pltpu.VMEM((units, 2) + rows, bf16),
            pltpu.VMEM((units,) + rows, bf16),
            pltpu.VMEM((units,) + rows, bf16),
            pltpu.VMEM((units,) + rows, bf16),
            pltpu.VMEM((n,) + rows, bf16),
            pltpu.VMEM((tp * cap, units_hidden), bf16),
            dma((8,)),
            dma((2 + 3 * pieces,)),
            dma((2 + 3 * pieces,)),
            dma((planes,)),
            dma((planes,)),
            dma((2, planes)),
            dma((planes,)),
            dma((planes, 2)),
            dma((planes, 2)),
            dma((3, planes, 2, 2)),
            dma((3, planes, 2, 2)),
            dma((3, units)),
            dma((3, units)),
            dma((units, 2)),
            dma((n, 2)),
        ],
        compiler_params=pltpu.CompilerParams(
            collective_id=3, has_side_effects=True, vmem_limit_bytes=60 * 1024 * 1024
        ),
    )(
        routes.T, route_weight.T, conv_taps, norm_gain.reshape(1, width),
        gate_in, value_in, gate_out, proj_weight, residual,
        expert_gate[0], expert_up[0], expert_down[0],
    )


def body(*args):
    residual, routes = args[5], args[7]
    n, tp = lax.axis_size("sp"), lax.axis_size("tp")
    quarter = residual.shape[0]
    capacity = 2 * quarter * routes.shape[1] // n
    relay = n % 2 == 0 and tp == 4 and capacity % 32 == 0 and quarter % 128 == 0
    if relay and (n // 2) * quarter <= n * capacity:
        return relay_body(*args)
    return exchange_body(*args)


def solution(mesh):
    placed = (
        P("sp", "tp"),
        P("sp", "tp"),
        P("sp", "tp"),
        P(None, "tp"),
        P("tp", None),
        P(("sp", "tp"), None),
        P(),
        P("sp", None),
        P("sp", None),
        P("sp", None, "tp"),
        P("sp", None, "tp"),
        P("sp", "tp", None),
    )
    return jax.shard_map(
        body, mesh=mesh, in_specs=placed, out_specs=P(("sp", "tp"), None), check_vma=False
    )
```

profile of v0, /device:TPU:0, one launch (start us, length us, event | category | flops | bytes accessed | tf_op | source)
XLA Modules:
  0.0 148.2 jit_solution(18423642343313979052)
XLA Ops:
  0.0 146.3 %shard_map.118 = bf16[128,2048]{1,0:T(8,128)(2,1)} custom-call(s32[2,512]{1,0:T(2,128)} %bitcast.10, f32[2,512]{1,0:T(2,128)} %bitcast.11, f32[3,512]{1,0:T(4,128)} %taps_ref.1, f32[1,2048]{1,0:T(1,128)} %bitcast.9, bf16[512,512]{1,0:T(8,128)(2,1)} %gate_hbm.1, bf16[512,512]{1,0:T(8,128)(2,1)} %value_hbm.1, bf16[512,512]{1,0:T(8,128)(2,1)} %out_gate_hbm.1, ...), custom_call_target="tpu_custom_call" | custom-call | tf_op jit(solution)/shard_map/pallas_call | solution.py:903
  146.3 1.9 %copy.14 = bf16[128,2048]{1,0:T(8,128)(2,1)} copy(bf16[128,2048]{1,0:T(8,128)(2,1)} %shard_map.118) | data formatting | bytes 1048576
where the time goes:
time: 149 us; the launch traced here: 148 us
  Pallas kernels  146 us (98%)
  local copies, waits for them, and re-layouts  1.88 us (1%)
    pallas_call x1, Pallas kernels, relay_body(): pl.pallas_call(functools.partial(layer_kernel, n, tp, halo, pieces, cap),...  146 us

commit v1 on v0

--- a/solution.py
+++ b/solution.py
@@ -428,11 +428,7 @@
 
 
 def plane_of(j, z, planes):
-    upper = z >= planes // 2
-    near = jnp.where(upper, planes - 1 - z, z)
-    swing = jnp.where(j % 2 == 1, near - (j + 1) // 2, near + j // 2)
-    place = jnp.where(j <= 2 * near, swing, j)
-    return jnp.where(upper, planes - 1 - place, place)
+    return jnp.where(z < planes // 2, z + j, z + planes - j) % planes
 
 
 def layer_kernel(
@@ -455,7 +451,6 @@
     mate_across = (mate + 2) % tp
     tokens = gate_ref.shape[0]
     quarter, width = res_ref.shape
-    piece = quarter // pieces
     half = cap // 2
     units = 2 * planes
     after, before = (s + 1) % n, (s + n - 1) % n
@@ -504,8 +499,6 @@
         name.astype(f32) * cap + jnp.sum(count * hot, axis=0, keepdims=True)
         for name, hot in zip(named, one_hot)
     ]
-    info[z] = jnp.concatenate(picks + [jnp.zeros((6, quarter), f32)], axis=0)
-
     for copy in loads[:2]:
         copy.wait()
     tail = pl.ds(tokens - halo, halo)
@@ -525,31 +518,36 @@
         origin = (z + k) % planes
         return remote(info.at[origin], info.at[origin], isend.at[k], igot.at[origin], (s, mate))
 
-    @pl.loop(1, planes)
-    def _(k):
-        tell(k).start()
-
     for copy in loads[5:]:
         copy.start()
 
-    body_rows = pl.ds(halo, tokens)
-    product[body_rows] = gate_ref[...].astype(f32) * value_ref[...].astype(f32)
-    for copy in edges:
-        copy.wait_recv()
-    prior = edge[0].astype(f32) * edge[1].astype(f32)
-    product[pl.ds(0, halo)] = jnp.where(s == 0, 0.0, prior)
-    conv_sum = (
-        taps_ref[0:1] * product[pl.ds(halo - 2, tokens)]
-        + taps_ref[1:2] * product[pl.ds(halo - 1, tokens)]
-        + taps_ref[2:3] * product[body_rows]
-    )
+    product[pl.ds(halo, tokens)] = gate_ref[...].astype(f32) * value_ref[...].astype(f32)
     loads[2].wait()
-    mixed[...] = (out_gate_ref[...].astype(f32) * conv_sum).astype(bf16)
-    loads[3].wait()
+    part_width = width // pieces
+
+    def mix(block):
+        @pl.when(block == 0)
+        def _():
+            for copy in edges:
+                copy.wait_recv()
+            prior = edge[0].astype(f32) * edge[1].astype(f32)
+            product[pl.ds(0, halo)] = jnp.where(s == 0, 0.0, prior)
+
+        at = pl.ds(pl.multiple_of(block * quarter, quarter), quarter)
+        window = product[pl.ds(pl.multiple_of(block * quarter, quarter), halo + quarter)]
+        conv_sum = (
+            taps_ref[0:1] * window[halo - 2:halo - 2 + quarter]
+            + taps_ref[1:2] * window[halo - 1:halo - 1 + quarter]
+            + taps_ref[2:3] * window[halo:]
+        )
+        mixed[at] = (out_gate_ref[at].astype(f32) * conv_sum).astype(bf16)
+
+    def columns(p):
+        return pl.ds(p * part_width, part_width)
 
     def project(block, p):
-        first = pl.multiple_of(block * quarter + p * piece, piece)
-        y_block = jnp.dot(mixed[pl.ds(first, piece)], proj_ref[...], preferred_element_type=f32)
+        at = pl.ds(pl.multiple_of(block * quarter, quarter), quarter)
+        y_block = jnp.dot(mixed[at], proj_ref[:, columns(p)], preferred_element_type=f32)
         mpart[block, p] = y_block.astype(bf16)
 
     def lane(kind, p):
@@ -563,17 +561,25 @@
         at = lane(2, p)
         return remote(msum.at[p], mfar.at[p], msend.at[at], mgot.at[at], (s, across))
 
-    for p in range(pieces):
+    mix(mate_across)
+    loads[3].wait()
+    for p in range(min(2, pieces)):
         project(mate_across, p)
         to_mate(0, mate_across, p).start()
+    mix(across)
     for p in range(pieces):
         project(across, p)
         to_mate(0, mate_across, p).wait_recv()
         msum[p] = (mpart[across, p].astype(f32) + mmate[0, p].astype(f32)).astype(bf16)
         to_across(p).start()
+        if p + 2 < pieces:
+            project(mate_across, p + 2)
+            to_mate(0, mate_across, p + 2).start()
+    mix(mate)
     for p in range(pieces):
         project(mate, p)
         to_mate(1, mate, p).start()
+    mix(t)
     for p in range(pieces):
         project(t, p)
 
@@ -586,37 +592,49 @@
     spread[0] = high
     spread[1] = (share - high.astype(f32)).astype(bf16)
 
+    def along(block, up, at=slice(None)):
+        to = jnp.where(up == 1, z + 1, z - 1)
+        ref = raw.at[block, :, at]
+        return remote(ref, ref, rsend.at[up, block], rgot.at[block], (to * 2 + y, t))
+
+    def has_up(block):
+        return (block <= z) & (z < planes - 1)
+
+    def has_down(block):
+        return (block >= z) & (z > 0)
+
+    def pass_on(block):
+        @pl.when(has_up(block))
+        def _():
+            along(block, 1).start()
+
+        @pl.when(has_down(block))
+        def _():
+            along(block, 0).start()
+
     loads[4].wait()
+    square = jnp.zeros((quarter, 1), f32)
     for p in range(pieces):
+        at = columns(p)
         to_mate(1, mate, p).wait_recv()
         to_across(p).wait_recv()
-        at = pl.ds(p * piece, piece)
-        summed = (
-            mpart[t, p].astype(f32) + mmate[1, p].astype(f32) + mfar[p].astype(f32)
-        )
-        hidden_rows = res_ref[at].astype(f32) + summed
-        inverse = lax.rsqrt(jnp.mean(hidden_rows * hidden_rows, axis=-1, keepdims=True) + 1e-05)
-        rows[at] = hidden_rows
-        raw[z, at] = (hidden_rows * inverse * gain_ref[...]).astype(bf16)
-
-    def along(block, up):
-        to = jnp.where(up == 1, z + 1, z - 1)
-        return remote(raw.at[block], raw.at[block], rsend.at[up, block], rgot.at[block], (to * 2 + y, t))
-
-    def has_up(block):
-        return (block <= z) & (z < planes - 1)
-
-    def has_down(block):
-        return (block >= z) & (z > 0)
-
-    def pass_on(block):
-        @pl.when(has_up(block))
-        def _():
-            along(block, 1).start()
-
-        @pl.when(has_down(block))
-        def _():
-            along(block, 0).start()
+        summed = mpart[t, p].astype(f32) + mmate[1, p].astype(f32) + mfar[p].astype(f32)
+        hidden_rows = res_ref[:, at].astype(f32) + summed
+        rows[:, at] = hidden_rows
+        raw[z, :, at] = (hidden_rows * gain_ref[:, at]).astype(bf16)
+        for up, has in ((1, has_up), (0, has_down)):
+            @pl.when(has(z))
+            def _():
+                along(z, up, at).start()
+
+        square = square + jnp.sum(hidden_rows * hidden_rows, axis=-1, keepdims=True)
+    inverse = lax.rsqrt(square / width + 1e-05)
+    scale = jnp.transpose(jnp.broadcast_to(inverse, (quarter, quarter)))[0:1]
+    info[z] = jnp.concatenate(picks + [scale, jnp.zeros((5, quarter), f32)], axis=0)
+
+    @pl.loop(1, planes)
+    def _(k):
+        tell(k).start()
 
     def beside(j, h):
         return remote(
@@ -642,23 +660,25 @@
             expert * cap
         ).astype(f32)
         table = info[block]
-        chosen = ((place == table[0:1]) | (place == table[1:2])).astype(f32).astype(bf16)
+        named = (place == table[0:1]) | (place == table[1:2])
+        chosen = named.astype(f32).astype(bf16)
+        scale = jnp.sum(jnp.where(named, table[2:3], 0.0), axis=1, keepdims=True)
 
         @pl.loop(0, width // wide)
         def _(c):
             at = pl.ds(pl.multiple_of(c * wide, wide), wide)
-            taken = jnp.dot(chosen, raw[block, :, at], preferred_element_type=f32).astype(bf16)
+            taken = jnp.dot(chosen, raw[block, :, at], preferred_element_type=f32)
+            taken = (taken * scale).astype(bf16)
             for h in range(2):
                 put(h, at, taken[h * half:(h + 1) * half])
 
+    def arrive(j):
+        block = plane_of(j, z, planes)
+        along(block, 1).wait_recv()
+        pass_on(block)
+
     def dispatch(j):
         block = plane_of(j, z, planes)
-
-        @pl.when(j > 0)
-        def _():
-            along(block, 1).wait_recv()
-
-        pass_on(block)
 
         @pl.when(j > 0)
         def _():
@@ -685,14 +705,10 @@
             over(j, h, other_y).start()
             pair_own(j, h, other_y).start()
 
-    def dispatch_far(j):
-        for source in (y, other_y):
-            for h in (1, 0):
-                over(j, h, source).wait_recv()
-                pair_far(j, h, source).start()
-
-    def group(u):
-        return (u + 1) // 2 % planes, (u + 1) % 2
+    def dispatch_far(j, source):
+        for h in (1, 0):
+            over(j, h, source).wait_recv()
+            pair_far(j, h, source).start()
 
     def part_near(u):
         return remote(part.at[u, mate], mrecv.at[u, 0], psend.at[0, u], pgot.at[0, u], (s, mate))
@@ -703,8 +719,8 @@
     def sum_over(u):
         return remote(psum.at[u], xrecv.at[u], psend.at[2, u], pgot.at[2, u], (s, across))
 
-    def ffn(u):
-        j, h = group(u)
+    def ffn(j, h):
+        u = 2 * j + h
         for source in range(2):
             pair_own(j, h, source).wait_recv()
             pair_far(j, h, source).wait_recv()
@@ -728,21 +744,22 @@
         part_far(u).start()
         part_near(u).start()
 
-    def homeward(u, source):
-        j, h = group(u)
+    def homeward(j, h, source):
+        u = 2 * j + h
         to = plane_of(j, z, planes) * 2 + source
         return remote(fin.at[u, source], ret.at[s, h], hsend.at[u, source], hgot.at[s, h], (to, t))
 
     def returned(origin, h):
         return remote(ret.at[origin, h], ret.at[origin, h], hsend.at[0, 0], hgot.at[origin, h], (s, mate))
 
-    def sum_far(u):
+    def sum_far(j, h):
+        u = 2 * j + h
         part_far(u).wait_recv()
         psum[u] = (part[u, across].astype(f32) + mrecv[u, 1].astype(f32)).astype(bf16)
         sum_over(u).start()
 
-    def send_home(u):
-        j, h = group(u)
+    def send_home(j, h):
+        u = 2 * j + h
         part_near(u).wait_recv()
         sum_over(u).wait_recv()
         total = (
@@ -753,59 +770,12 @@
         @pl.when(j == 0)
         def _():
             ret[s, h] = fin[u, y]
-            homeward(u, other_y).start()
+            homeward(j, h, other_y).start()
 
         @pl.when(j > 0)
         def _():
             for source in range(2):
-                homeward(u, source).start()
-
-    dispatch(0)
-    dispatch_beside(0)
-    for copy in loads[5:]:
-        copy.wait()
-
-    @pl.loop(0, planes + 1)
-    def _(j):
-        @pl.when(j + 1 < planes)
-        def _():
-            dispatch(j + 1)
-
-        @pl.when(j < planes)
-        def _():
-            dispatch_far(j)
-
-        first = 2 * j - 1
-
-        @pl.when(j > 0)
-        def _():
-            ffn(first)
-
-        @pl.when(j + 1 < planes)
-        def _():
-            dispatch_beside(j + 1)
-
-        @pl.when(j < planes)
-        def _():
-            ffn(2 * j)
-
-        @pl.when(j > 0)
-        def _():
-            sum_far(first)
-
-        @pl.when(j > 1)
-        def _():
-            send_home(first - 2)
-
-        @pl.when(j > 0)
-        def _():
-            send_home(first - 1)
-
-        @pl.when(j < planes)
-        def _():
-            sum_far(2 * j)
-
-    send_home(units - 1)
+                homeward(j, h, source).start()
 
     def gather(plane, put):
         for source in range(2):
@@ -835,10 +805,87 @@
     def finish(at, value):
         out_ref[:, at] = value.astype(bf16)
 
-    @pl.loop(1, planes)
+    at_end = (z == 0) | (z == planes - 1)
+    late = jnp.where(at_end, 1, 0)
+
+    dispatch(0)
+    arrive(1)
+
+    @pl.when(late == 0)
+    def _():
+        arrive(planes - 1)
+
+    dispatch_beside(0)
+    for copy in loads[5:]:
+        copy.wait()
+
+    @pl.loop(0, planes)
     def _(j):
-        gather(plane_of(j, z, planes), keep)
-
+        @pl.when((j > 0) & (late == 1) & (j + 1 < planes))
+        def _():
+            arrive(j + 1)
+
+        @pl.when(j + 1 < planes)
+        def _():
+            dispatch(j + 1)
+
+        dispatch_far(j, y)
+
+        @pl.when(j > 1 + late)
+        def _():
+            send_home(j - 1, 0)
+
+        dispatch_far(j, other_y)
+        ffn(j, 0)
+
+        @pl.when(j > late)
+        def _():
+            sum_far(j, 0)
+
+        @pl.when(j == 0)
+        def _():
+            dispatch_beside(1)
+
+        @pl.when((j == 0) & (late == 0))
+        def _():
+            arrive(2)
+
+        ffn(j, 1)
+
+        @pl.when(j > 1 + late)
+        def _():
+            send_home(j - 1, 1)
+
+        @pl.when((j > 0) & (j + 1 < planes))
+        def _():
+            dispatch_beside(j + 1)
+
+        @pl.when(j > late)
+        def _():
+            sum_far(j, 1)
+
+    @pl.when(late == 1)
+    def _():
+        sum_far(1, 0)
+        sum_far(1, 1)
+
+    sum_far(0, 0)
+    sum_far(0, 1)
+    send_home(planes - 1, 0)
+    send_home(planes - 1, 1)
+
+    @pl.when(late == 1)
+    def _():
+        send_home(1, 0)
+        send_home(1, 1)
+
+    @pl.loop(1, planes - 1)
+    def _(j):
+        gather(plane_of(j + late, z, planes), keep)
+
+    send_home(0, 0)
+    send_home(0, 1)
+    gather(plane_of(jnp.where(late == 1, 1, planes - 1), z, planes), keep)
     gather(z, finish)
 
     for copy in edges:
@@ -874,12 +921,11 @@
         part_near(u).wait_send()
         part_far(u).wait_send()
         sum_over(u).wait_send()
-        j, h = group(u)
-        homeward(u, other_y).wait_send()
-
-        @pl.when(j > 0)
-        def _():
-            homeward(u, y).wait_send()
+        homeward(u // 2, u % 2, other_y).wait_send()
+
+        @pl.when(u > 1)
+        def _():
+            homeward(u // 2, u % 2, y).wait_send()
 
 
 def relay_body(
@@ -894,7 +940,7 @@
     planes, half = n // 2, cap // 2
     units = 2 * planes
     halo, pieces = 16, 4
-    piece = quarter // pieces
+    part_width = width // pieces
     vmem = pl.BlockSpec(memory_space=pltpu.VMEM)
     hbm = pl.BlockSpec(memory_space=pl.ANY)
     bf16, f32 = jnp.bfloat16, jnp.float32
@@ -917,10 +963,10 @@
             pltpu.VMEM((2, halo, channels), bf16),
             pltpu.VMEM((halo + tokens, channels), f32),
             pltpu.VMEM((tokens, channels), bf16),
-            pltpu.VMEM((tp, pieces, piece, width), bf16),
-            pltpu.VMEM((2, pieces, piece, width), bf16),
-            pltpu.VMEM((pieces, piece, width), bf16),
-            pltpu.VMEM((pieces, piece, width), bf16),
+            pltpu.VMEM((tp, pieces, quarter, part_width), bf16),
+            pltpu.VMEM((2, pieces, quarter, part_width), bf16),
+            pltpu.VMEM((pieces, quarter, part_width), bf16),
+            pltpu.VMEM((pieces, quarter, part_width), bf16),
             pltpu.VMEM((quarter, width), f32),
             pltpu.VMEM((planes, 8, quarter), f32),
             pltpu.VMEM((2, quarter, n * cap), bf16),
@@ -965,7 +1011,7 @@
     n, tp = lax.axis_size("sp"), lax.axis_size("tp")
     quarter = residual.shape[0]
     capacity = 2 * quarter * routes.shape[1] // n
-    relay = n % 2 == 0 and tp == 4 and capacity % 32 == 0 and quarter % 128 == 0
+    relay = n == 2 * tp and tp == 4 and capacity % 32 == 0 and quarter % 128 == 0
     if relay and (n // 2) * quarter <= n * capacity:
         return relay_body(*args)
     return exchange_body(*args)

time: 149 us -> 134 us (0.90)
  Pallas kernels: 146 us -> 132 us
    pallas_call x1, Pallas kernels: 146 us -> 132 us  [relay_body(): pl.pallas_call(functools.partial(layer_kernel, n, tp, halo, pieces, cap),...]
where the time goes in v1:
time: 134 us; the launch traced here: 133 us
  Pallas kernels  132 us (99%)
  local copies, waits for them, and re-layouts  1.88 us (1%)
    pallas_call x1, Pallas kernels, relay_body(): pl.pallas_call(functools.partial(layer_kernel, n, tp, halo, pieces, cap),...  132 us

profile of v1, /device:TPU:0, one launch (start us, length us, event | category | flops | bytes accessed | tf_op | source)
XLA Modules:
  0.0 133.4 jit_solution(670452128046384924)
XLA Ops:
  0.0 131.6 %shard_map.118 = bf16[128,2048]{1,0:T(8,128)(2,1)} custom-call(s32[2,512]{1,0:T(2,128)} %bitcast.10, f32[2,512]{1,0:T(2,128)} %bitcast.11, f32[3,512]{1,0:T(4,128)} %taps_ref.1, f32[1,2048]{1,0:T(1,128)} %bitcast.9, bf16[512,512]{1,0:T(8,128)(2,1)} %gate_hbm.1, bf16[512,512]{1,0:T(8,128)(2,1)} %value_hbm.1, bf16[512,512]{1,0:T(8,128)(2,1)} %out_gate_hbm.1, ...), custom_call_target="tpu_custom_call" | custom-call | tf_op jit(solution)/shard_map/pallas_call | solution.py:949
  131.6 1.9 %copy.14 = bf16[128,2048]{1,0:T(8,128)(2,1)} copy(bf16[128,2048]{1,0:T(8,128)(2,1)} %shard_map.118) | data formatting | bytes 1048576

commit v2 on v1

--- a/solution.py
+++ b/solution.py
@@ -432,14 +432,15 @@
 
 
 def layer_kernel(
-    n, tp, halo, pieces, cap,
+    n, tp, halo, pieces, cap, early,
     routes_ref, weights_ref, taps_ref, gain_ref,
     gate_hbm, value_hbm, out_gate_hbm, proj_hbm, res_hbm, wg_hbm, wu_hbm, wd_hbm,
     out_ref,
     gate_ref, value_ref, out_gate_ref, proj_ref, res_ref, gate_w, up_w, down_w,
     edge, product, mixed, mpart, mmate, msum, mfar,
-    rows, info, spread, raw, ysend, recv, part, mrecv, psum, xrecv, fin, ret, hid,
+    rows, info, far_info, spread, raw, far_raw, ysend, far_ysend, recv, part, mrecv, psum, xrecv, fin, ret, hid,
     local_sem, msend, mgot, isend, igot, rsend, rgot, ysem, ygot, dsend, dgot, psend, pgot, hsend, hgot,
+    csend, fisend, figot, frsend, frgot, fysem, fygot,
 ):
     s = lax.axis_index("sp")
     t = lax.axis_index("tp")
@@ -475,6 +476,11 @@
     def _(k):
         pl.semaphore_signal(barrier, inc=1, device_id=((s + k) % n, t), device_id_type=MESH)
 
+    @pl.loop(1, planes)
+    def _(k):
+        to = (z + k) % planes * 2 + y
+        pl.semaphore_signal(barrier, inc=1, device_id=(to, across), device_id_type=MESH)
+
     for peer in (mate, across):
         pl.semaphore_signal(barrier, inc=1, device_id=(s, peer), device_id_type=MESH)
 
@@ -499,17 +505,6 @@
         name.astype(f32) * cap + jnp.sum(count * hot, axis=0, keepdims=True)
         for name, hot in zip(named, one_hot)
     ]
-    for copy in loads[:2]:
-        copy.wait()
-    tail = pl.ds(tokens - halo, halo)
-    edges = [
-        remote(ref.at[tail], edge.at[i], msend.at[i], mgot.at[i], (after, t))
-        for i, ref in enumerate((gate_ref, value_ref))
-    ]
-    pl.semaphore_wait(barrier, n + 1)
-    for copy in edges:
-        copy.start()
-
     def tell(k):
         to = (z + k) % planes
         return remote(info.at[z], info.at[z], isend.at[k], igot.at[z], (to * 2 + y, t))
@@ -521,18 +516,21 @@
     for copy in loads[5:]:
         copy.start()
 
+    def tell_far(k):
+        to = (z + k) % planes
+        return remote(info.at[z], far_info.at[z], fisend.at[k], figot.at[z], (to * 2 + y, across))
+
+    def told_far(origin):
+        ref = far_info.at[origin]
+        return remote(ref, ref, fisend.at[0], figot.at[origin], (s, mate))
+
+    for copy in loads[:2]:
+        copy.wait()
     product[pl.ds(halo, tokens)] = gate_ref[...].astype(f32) * value_ref[...].astype(f32)
     loads[2].wait()
     part_width = width // pieces
 
     def mix(block):
-        @pl.when(block == 0)
-        def _():
-            for copy in edges:
-                copy.wait_recv()
-            prior = edge[0].astype(f32) * edge[1].astype(f32)
-            product[pl.ds(0, halo)] = jnp.where(s == 0, 0.0, prior)
-
         at = pl.ds(pl.multiple_of(block * quarter, quarter), quarter)
         window = product[pl.ds(pl.multiple_of(block * quarter, quarter), halo + quarter)]
         conv_sum = (
@@ -542,6 +540,10 @@
         )
         mixed[at] = (out_gate_ref[at].astype(f32) * conv_sum).astype(bf16)
 
+    @pl.loop(1, tp)
+    def _(block):
+        mix(block)
+
     def columns(p):
         return pl.ds(p * part_width, part_width)
 
@@ -550,6 +552,31 @@
         y_block = jnp.dot(mixed[at], proj_ref[:, columns(p)], preferred_element_type=f32)
         mpart[block, p] = y_block.astype(bf16)
 
+    loads[3].wait()
+    opens = mate_across == 0
+    ahead = jnp.where(opens, across, mate_across)
+    for p in range(pieces):
+        project(ahead, p)
+
+    tail = pl.ds(tokens - halo, halo)
+    edges = [
+        remote(ref.at[tail], edge.at[i], msend.at[i], mgot.at[i], (after, t))
+        for i, ref in enumerate((gate_ref, value_ref))
+    ]
+    pl.semaphore_wait(barrier, n + planes)
+    for copy in edges:
+        copy.start()
+
+
+    def first_block(block):
+        @pl.when(block == 0)
+        def _():
+            for copy in edges:
+                copy.wait_recv()
+            prior = edge[0].astype(f32) * edge[1].astype(f32)
+            product[pl.ds(0, halo)] = jnp.where(s == 0, 0.0, prior)
+            mix(block)
+
     def lane(kind, p):
         return 2 + kind * pieces + p
 
@@ -561,25 +588,34 @@
         at = lane(2, p)
         return remote(msum.at[p], mfar.at[p], msend.at[at], mgot.at[at], (s, across))
 
-    mix(mate_across)
-    loads[3].wait()
-    for p in range(min(2, pieces)):
-        project(mate_across, p)
-        to_mate(0, mate_across, p).start()
-    mix(across)
-    for p in range(pieces):
-        project(across, p)
+    def cross_sum(p):
         to_mate(0, mate_across, p).wait_recv()
         msum[p] = (mpart[across, p].astype(f32) + mmate[0, p].astype(f32)).astype(bf16)
         to_across(p).start()
-        if p + 2 < pieces:
-            project(mate_across, p + 2)
-            to_mate(0, mate_across, p + 2).start()
-    mix(mate)
+
+    @pl.when(opens)
+    def _():
+        for p in range(pieces):
+            cross_sum(p)
+        first_block(mate_across)
+        for p in range(pieces):
+            project(mate_across, p)
+            to_mate(0, mate_across, p).start()
+
+    @pl.when(jnp.logical_not(opens))
+    def _():
+        for p in range(pieces):
+            to_mate(0, mate_across, p).start()
+        first_block(across)
+        for p in range(pieces):
+            project(across, p)
+            cross_sum(p)
+
+    first_block(mate)
     for p in range(pieces):
         project(mate, p)
         to_mate(1, mate, p).start()
-    mix(t)
+    first_block(t)
     for p in range(pieces):
         project(t, p)
 
@@ -611,6 +647,18 @@
         @pl.when(has_down(block))
         def _():
             along(block, 0).start()
+
+    first_columns, last_columns = pl.ds(0, early), pl.ds(early, width - early)
+
+    def cross():
+        return remote(
+            raw.at[z, :, first_columns], far_raw.at[z], csend.at[0], frgot.at[z], (s, across)
+        )
+
+    def along_far(block, up):
+        to = jnp.where(up == 1, z + 1, z - 1)
+        ref = far_raw.at[block]
+        return remote(ref, ref, frsend.at[up, block], frgot.at[block], (to * 2 + y, t))
 
     loads[4].wait()
     square = jnp.zeros((quarter, 1), f32)
@@ -627,6 +675,8 @@
             def _():
                 along(z, up, at).start()
 
+        if p == (early - 1) // part_width:
+            cross().start()
         square = square + jnp.sum(hidden_rows * hidden_rows, axis=-1, keepdims=True)
     inverse = lax.rsqrt(square / width + 1e-05)
     scale = jnp.transpose(jnp.broadcast_to(inverse, (quarter, quarter)))[0:1]
@@ -636,13 +686,23 @@
     def _(k):
         tell(k).start()
 
+    @pl.loop(0, planes)
+    def _(k):
+        tell_far(k).start()
+
     def beside(j, h):
         return remote(
             ysend.at[j, h], recv.at[j, h, t, y], ysem.at[j, h], ygot.at[j, h], (z * 2 + other_y, t)
         )
 
+    def beside_far(j, h):
+        return remote(
+            far_ysend.at[j, h], recv.at[j, h, across, y, :, first_columns],
+            fysem.at[j, h], fygot.at[j, h], (z * 2 + other_y, t),
+        )
+
     def over(j, h, source):
-        ref = recv.at[j, h, t, source]
+        ref = recv.at[j, h, t, source, :, last_columns]
         return remote(ref, ref, dsend.at[0, j, h, source], dgot.at[0, j, h, source], (s, across))
 
     def pair_own(j, h, source):
@@ -655,7 +715,7 @@
 
     wide = min(512, width)
 
-    def select(j, block, expert, put):
+    def select(raw, info, block, expert, put):
         place = lax.broadcasted_iota(jnp.int32, (cap, quarter), 0).astype(f32) + (
             expert * cap
         ).astype(f32)
@@ -664,50 +724,81 @@
         chosen = named.astype(f32).astype(bf16)
         scale = jnp.sum(jnp.where(named, table[2:3], 0.0), axis=1, keepdims=True)
 
-        @pl.loop(0, width // wide)
+        step = raw.shape[2] if raw.shape[2] % wide else wide
+
+        @pl.loop(0, raw.shape[2] // step)
         def _(c):
-            at = pl.ds(pl.multiple_of(c * wide, wide), wide)
+            at = pl.ds(pl.multiple_of(c * step, step), step)
             taken = jnp.dot(chosen, raw[block, :, at], preferred_element_type=f32)
             taken = (taken * scale).astype(bf16)
             for h in range(2):
                 put(h, at, taken[h * half:(h + 1) * half])
 
+    def arrive_far(j):
+        block = plane_of(j, z, planes)
+        along_far(block, 1).wait_recv()
+
+        @pl.when(has_up(block))
+        def _():
+            along_far(block, 1).start()
+
+        @pl.when(has_down(block))
+        def _():
+            along_far(block, 0).start()
+
+    def dispatch_early(j):
+        block = plane_of(j, z, planes)
+        told_far(block).wait_recv()
+
+        def put_own(h, at, value):
+            recv[j, h, across, y, :, at] = value
+
+        def put_other(h, at, value):
+            far_ysend[j, h, :, at] = value
+
+        select(far_raw, far_info, block, z * 2 + other_y, put_other)
+        for h in range(2):
+            beside_far(j, h).start()
+        select(far_raw, far_info, block, s, put_own)
+
     def arrive(j):
         block = plane_of(j, z, planes)
         along(block, 1).wait_recv()
         pass_on(block)
 
-    def dispatch(j):
-        block = plane_of(j, z, planes)
-
+    def hear(j):
         @pl.when(j > 0)
         def _():
-            told((block + planes - z) % planes).wait_recv()
-
-        def put_own(h, at, value):
+            told((plane_of(j, z, planes) + planes - z) % planes).wait_recv()
+
+    def dispatch_own(j):
+        def put(h, at, value):
             recv[j, h, t, y, :, at] = value
 
-        def put_other(h, at, value):
+        select(raw, info, plane_of(j, z, planes), s, put)
+        for h in range(2):
+            over(j, h, y).start()
+            pair_own(j, h, y).start()
+
+    def dispatch_other(j):
+        def put(h, at, value):
             ysend[j, h, :, at] = value
 
-        select(j, block, s, put_own)
-        for h in (1, 0):
-            over(j, h, y).start()
-        select(j, block, z * 2 + other_y, put_other)
-        for h in (1, 0):
+        select(raw, info, plane_of(j, z, planes), z * 2 + other_y, put)
+        for h in range(2):
             beside(j, h).start()
-        for h in (1, 0):
-            pair_own(j, h, y).start()
 
     def dispatch_beside(j):
-        for h in (1, 0):
+        for h in range(2):
             beside(j, h).wait_recv()
             over(j, h, other_y).start()
             pair_own(j, h, other_y).start()
 
-    def dispatch_far(j, source):
-        for h in (1, 0):
+    def dispatch_far(j, source, crossed):
+        for h in range(2):
             over(j, h, source).wait_recv()
+            if crossed:
+                beside_far(j, h).wait_recv()
             pair_far(j, h, source).start()
 
     def part_near(u):
@@ -808,86 +899,114 @@
     at_end = (z == 0) | (z == planes - 1)
     late = jnp.where(at_end, 1, 0)
 
-    dispatch(0)
-    arrive(1)
+    def far_near(j):
+        dispatch_far(j, y, False)
+
+    def far_other(j):
+        dispatch_far(j, other_y, True)
+
+    def home_pair(j):
+        send_home(j, 0)
+        send_home(j, 1)
+
+    def take(j):
+        hear(j)
+        dispatch_own(j)
+        dispatch_other(j)
+
+    last = planes - 1
+    middle_start = [
+        (dispatch_own, 0), (arrive_far, 0), (arrive, 1), (arrive, last), (hear, 1),
+        (dispatch_other, 1), (dispatch_own, 1), (arrive_far, 1), (arrive_far, last),
+        (dispatch_early, 1), (hear, last), (dispatch_other, last), (dispatch_early, last),
+        (far_near, 1), (dispatch_beside, 1), (dispatch_own, last), (dispatch_other, 0),
+        (dispatch_early, 0), (far_other, 1),
+    ]
+    middle_after = [
+        [
+            (arrive, 2), (sum_far, 1, 0), (dispatch_beside, last), (take, 2), (arrive_far, 2),
+            (dispatch_early, 2),
+        ],
+        [(sum_far, 1, 1), (send_home, 1, 0), (far_near, last), (far_other, last), (dispatch_beside, 2)],
+        [(sum_far, last, 0), (far_near, 2), (send_home, 1, 1), (far_other, 2)],
+        [(sum_far, 2, 0), (send_home, last, 0)],
+        [(sum_far, last, 1), (dispatch_beside, 0)],
+        [
+            (send_home, 2, 0), (sum_far, 2, 1), (far_near, 0), (send_home, last, 1),
+            (far_other, 0),
+        ],
+        [(sum_far, 0, 0)],
+        [(sum_far, 0, 1), (send_home, 2, 1)],
+    ]
+    end_start = [
+        (dispatch_own, 0), (dispatch_other, 0), (arrive_far, 0), (arrive, 1), (dispatch_early, 0),
+        (dispatch_beside, 0), (take, 1), (arrive_far, 1), (dispatch_early, 1),
+        (far_near, 0), (far_other, 0),
+    ]
+    end_after = [
+        [(sum_far, 0, 0), (dispatch_beside, 1)],
+        [
+            (arrive, 2), (take, 2), (arrive_far, 2), (dispatch_early, 2),
+            (far_near, 1), (far_other, 1),
+        ],
+        [(dispatch_beside, 2)],
+        [
+            (sum_far, 1, 0), (arrive, last), (take, last), (arrive_far, last),
+            (dispatch_early, last), (far_near, 2), (far_other, 2),
+        ],
+        [(sum_far, 2, 0), (send_home, 1, 0), (dispatch_beside, last)],
+        [(sum_far, 2, 1), (far_near, last), (send_home, 2, 0), (far_other, last)],
+        [(sum_far, last, 0)],
+        [
+            (send_home, 2, 1), (sum_far, last, 1), (sum_far, 1, 1), (sum_far, 0, 1),
+            (send_home, 0, 0), (send_home, last, 0), (send_home, last, 1), (send_home, 1, 1),
+        ],
+    ]
+
+    def carry_out(actions):
+        for act, *where in actions:
+            act(*[jnp.int32(place) for place in where])
 
     @pl.when(late == 0)
     def _():
-        arrive(planes - 1)
-
-    dispatch_beside(0)
+        carry_out(middle_start)
+
+    @pl.when(late == 1)
+    def _():
+        carry_out(end_start)
+
     for copy in loads[5:]:
         copy.wait()
 
-    @pl.loop(0, planes)
-    def _(j):
-        @pl.when((j > 0) & (late == 1) & (j + 1 < planes))
-        def _():
-            arrive(j + 1)
-
-        @pl.when(j + 1 < planes)
-        def _():
-            dispatch(j + 1)
-
-        dispatch_far(j, y)
-
-        @pl.when(j > 1 + late)
-        def _():
-            send_home(j - 1, 0)
-
-        dispatch_far(j, other_y)
-        ffn(j, 0)
-
-        @pl.when(j > late)
-        def _():
-            sum_far(j, 0)
-
-        @pl.when(j == 0)
-        def _():
-            dispatch_beside(1)
-
-        @pl.when((j == 0) & (late == 0))
-        def _():
-            arrive(2)
-
-        ffn(j, 1)
-
-        @pl.when(j > 1 + late)
-        def _():
-            send_home(j - 1, 1)
-
-        @pl.when((j > 0) & (j + 1 < planes))
-        def _():
-            dispatch_beside(j + 1)
-
-        @pl.when(j > late)
-        def _():
-            sum_far(j, 1)
+    @pl.loop(0, units)
+    def _(k):
+        woven = (k > 1) & (k < units - 2)
+        middle_plane = jnp.where(k < 2, 1, jnp.where(woven, jnp.where(k % 2 == 0, last, 2), 0))
+        middle_half = jnp.where(woven, k // planes, k % 2)
+        ffn(jnp.where(late == 1, k // 2, middle_plane), jnp.where(late == 1, k % 2, middle_half))
+        for step in range(units):
+            @pl.when((k == step) & (late == 0))
+            def _():
+                carry_out(middle_after[step])
+
+            @pl.when((k == step) & (late == 1))
+            def _():
+                carry_out(end_after[step])
 
     @pl.when(late == 1)
     def _():
-        sum_far(1, 0)
-        sum_far(1, 1)
-
-    sum_far(0, 0)
-    sum_far(0, 1)
-    send_home(planes - 1, 0)
-    send_home(planes - 1, 1)
-
-    @pl.when(late == 1)
-    def _():
-        send_home(1, 0)
-        send_home(1, 1)
+        send_home(jnp.int32(0), jnp.int32(1))
 
     @pl.loop(1, planes - 1)
     def _(j):
         gather(plane_of(j + late, z, planes), keep)
 
-    send_home(0, 0)
-    send_home(0, 1)
+    @pl.when(late == 0)
+    def _():
+        send_home(jnp.int32(0), jnp.int32(0))
+        send_home(jnp.int32(0), jnp.int32(1))
+
     gather(plane_of(jnp.where(late == 1, 1, planes - 1), z, planes), keep)
-    gather(z, finish)
-
     for copy in edges:
         copy.wait_send()
     for p in range(pieces):
@@ -901,26 +1020,38 @@
         def _():
             tell(j).wait_send()
 
+        tell_far(j).wait_send()
+
         @pl.when(has_up(j))
         def _():
             along(j, 1).wait_send()
+            along_far(j, 1).wait_send()
 
         @pl.when(has_down(j))
         def _():
             along(j, 0).wait_send()
+            along_far(j, 0).wait_send()
 
         for h in range(2):
             beside(j, h).wait_send()
+            beside_far(j, h).wait_send()
             for source in range(2):
                 over(j, h, source).wait_send()
                 pair_own(j, h, source).wait_send()
                 pair_far(j, h, source).wait_send()
+
+    cross().wait_send()
 
     @pl.loop(0, units)
     def _(u):
         part_near(u).wait_send()
         part_far(u).wait_send()
         sum_over(u).wait_send()
+
+    gather(z, finish)
+
+    @pl.loop(0, units)
+    def _(u):
         homeward(u // 2, u % 2, other_y).wait_send()
 
         @pl.when(u > 1)
@@ -940,6 +1071,7 @@
     planes, half = n // 2, cap // 2
     units = 2 * planes
     halo, pieces = 16, 4
+    early = width // 1024 * 384
     part_width = width // pieces
     vmem = pl.BlockSpec(memory_space=pltpu.VMEM)
     hbm = pl.BlockSpec(memory_space=pl.ANY)
@@ -947,7 +1079,7 @@
     dma = pltpu.SemaphoreType.DMA
     rows = (2, half, width)
     return pl.pallas_call(
-        functools.partial(layer_kernel, n, tp, halo, pieces, cap),
+        functools.partial(layer_kernel, n, tp, halo, pieces, cap, early),
         out_shape=jax.ShapeDtypeStruct((quarter, width), bf16),
         in_specs=[vmem] * 4 + [hbm] * 8,
         out_specs=vmem,
@@ -969,9 +1101,12 @@
             pltpu.VMEM((pieces, quarter, part_width), bf16),
             pltpu.VMEM((quarter, width), f32),
             pltpu.VMEM((planes, 8, quarter), f32),
+            pltpu.VMEM((planes, 8, quarter), f32),
             pltpu.VMEM((2, quarter, n * cap), bf16),
             pltpu.VMEM((planes, quarter, width), bf16),
+            pltpu.VMEM((planes, quarter, early), bf16),
             pltpu.VMEM((planes,) + rows, bf16),
+            pltpu.VMEM((planes, 2, half, early), bf16),
             pltpu.VMEM((planes, 2, tp) + rows, bf16),
             pltpu.VMEM((units, tp) + rows, bf16),
             pltpu.VMEM((units, 2) + rows, bf16),
@@ -995,6 +1130,13 @@
             dma((3, units)),
             dma((units, 2)),
             dma((n, 2)),
+            dma((1,)),
+            dma((planes,)),
+            dma((planes,)),
+            dma((2, planes)),
+            dma((planes,)),
+            dma((planes, 2)),
+            dma((planes, 2)),
         ],
         compiler_params=pltpu.CompilerParams(
             collective_id=3, has_side_effects=True, vmem_limit_bytes=60 * 1024 * 1024
@@ -1011,7 +1153,7 @@
     n, tp = lax.axis_size("sp"), lax.axis_size("tp")
     quarter = residual.shape[0]
     capacity = 2 * quarter * routes.shape[1] // n
-    relay = n == 2 * tp and tp == 4 and capacity % 32 == 0 and quarter % 128 == 0
+    relay = n == 2 * tp and tp == 4 and capacity % 32 == 0 and quarter % 128 == 0 and residual.shape[1] % 1024 == 0
     if relay and (n // 2) * quarter <= n * capacity:
         return relay_body(*args)
     return exchange_body(*args)

time: 134 us -> 121 us (0.903)
  Pallas kernels: 132 us -> 118 us
    pallas_call x1, Pallas kernels: 132 us -> 118 us  [relay_body(): pl.pallas_call(functools.partial(layer_kernel, n, tp, halo, pieces, cap,...]
where the time goes in v2:
time: 121 us; the launch traced here: 120 us
  Pallas kernels  118 us (98%)
  local copies, waits for them, and re-layouts  1.88 us (2%)
    pallas_call x1, Pallas kernels, relay_body(): pl.pallas_call(functools.partial(layer_kernel, n, tp, halo, pieces, cap,...  118 us

profile of v2, /device:TPU:0, one launch (start us, length us, event | category | flops | bytes accessed | tf_op | source)
XLA Modules:
  0.0 119.8 jit_solution(16797951661299119127)
XLA Ops:
  0.0 117.9 %shard_map.118 = bf16[128,2048]{1,0:T(8,128)(2,1)} custom-call(s32[2,512]{1,0:T(2,128)} %bitcast.10, f32[2,512]{1,0:T(2,128)} %bitcast.11, f32[3,512]{1,0:T(4,128)} %taps_ref.1, f32[1,2048]{1,0:T(1,128)} %bitcast.9, bf16[512,512]{1,0:T(8,128)(2,1)} %gate_hbm.1, bf16[512,512]{1,0:T(8,128)(2,1)} %value_hbm.1, bf16[512,512]{1,0:T(8,128)(2,1)} %out_gate_hbm.1, ...), custom_call_target="tpu_custom_call" | custom-call | tf_op jit(solution)/shard_map/pallas_call | solution.py:1081
  117.9 1.9 %copy.14 = bf16[128,2048]{1,0:T(8,128)(2,1)} copy(bf16[128,2048]{1,0:T(8,128)(2,1)} %shard_map.118) | data formatting | bytes 1048576

commit v3 on v2

--- a/solution.py
+++ b/solution.py
@@ -438,7 +438,8 @@
     out_ref,
     gate_ref, value_ref, out_gate_ref, proj_ref, res_ref, gate_w, up_w, down_w,
     edge, product, mixed, mpart, mmate, msum, mfar,
-    rows, info, far_info, spread, raw, far_raw, ysend, far_ysend, recv, part, mrecv, psum, xrecv, fin, ret, hid,
+    rows, info, far_info, spread, raw, far_raw, ysend, far_ysend, recv, part, mrecv, psum, xrecv,
+    fin, ret, hid,
     local_sem, msend, mgot, isend, igot, rsend, rgot, ysem, ygot, dsend, dgot, psend, pgot, hsend, hgot,
     csend, fisend, figot, frsend, frgot, fysem, fygot,
 ):
@@ -692,26 +693,26 @@
 
     def beside(j, h):
         return remote(
-            ysend.at[j, h], recv.at[j, h, t, y], ysem.at[j, h], ygot.at[j, h], (z * 2 + other_y, t)
+            ysend.at[j, h], recv.at[j, h, t, y], ysem.at[0], ygot.at[j, h], (z * 2 + other_y, t)
         )
 
     def beside_far(j, h):
         return remote(
             far_ysend.at[j, h], recv.at[j, h, across, y, :, first_columns],
-            fysem.at[j, h], fygot.at[j, h], (z * 2 + other_y, t),
+            fysem.at[0], fygot.at[j, h], (z * 2 + other_y, t),
         )
 
     def over(j, h, source):
         ref = recv.at[j, h, t, source, :, last_columns]
-        return remote(ref, ref, dsend.at[0, j, h, source], dgot.at[0, j, h, source], (s, across))
+        return remote(ref, ref, dsend.at[0], dgot.at[0, j, h, source], (s, across))
 
     def pair_own(j, h, source):
         ref = recv.at[j, h, t, source]
-        return remote(ref, ref, dsend.at[1, j, h, source], dgot.at[1, j, h, source], (s, mate))
+        return remote(ref, ref, dsend.at[1], dgot.at[1, j, h, source], (s, mate))
 
     def pair_far(j, h, source):
         ref = recv.at[j, h, across, source]
-        return remote(ref, ref, dsend.at[2, j, h, source], dgot.at[2, j, h, source], (s, mate))
+        return remote(ref, ref, dsend.at[2], dgot.at[2, j, h, source], (s, mate))
 
     wide = min(512, width)
 
@@ -802,13 +803,13 @@
             pair_far(j, h, source).start()
 
     def part_near(u):
-        return remote(part.at[u, mate], mrecv.at[u, 0], psend.at[0, u], pgot.at[0, u], (s, mate))
+        return remote(part.at[u, mate], mrecv.at[u, 0], psend.at[0], pgot.at[0, u], (s, mate))
 
     def part_far(u):
-        return remote(part.at[u, mate_across], mrecv.at[u, 1], psend.at[1, u], pgot.at[1, u], (s, mate))
+        return remote(part.at[u, mate_across], mrecv.at[u, 1], psend.at[1], pgot.at[1, u], (s, mate))
 
     def sum_over(u):
-        return remote(psum.at[u], xrecv.at[u], psend.at[2, u], pgot.at[2, u], (s, across))
+        return remote(psum.at[u], xrecv.at[u], psend.at[2], pgot.at[2, u], (s, across))
 
     def ffn(j, h):
         u = 2 * j + h
@@ -816,7 +817,7 @@
             pair_own(j, h, source).wait_recv()
             pair_far(j, h, source).wait_recv()
         count = gate_w.shape[1]
-        cols = min(256, count)
+        cols = min(512, count)
 
         @pl.loop(0, count // cols)
         def _(c):
@@ -838,10 +839,10 @@
     def homeward(j, h, source):
         u = 2 * j + h
         to = plane_of(j, z, planes) * 2 + source
-        return remote(fin.at[u, source], ret.at[s, h], hsend.at[u, source], hgot.at[s, h], (to, t))
+        return remote(fin.at[u, source], ret.at[s, h], hsend.at[0], hgot.at[s, h], (to, t))
 
     def returned(origin, h):
-        return remote(ret.at[origin, h], ret.at[origin, h], hsend.at[0, 0], hgot.at[origin, h], (s, mate))
+        return remote(ret.at[origin, h], ret.at[origin, h], hsend.at[0], hgot.at[origin, h], (s, mate))
 
     def sum_far(j, h):
         u = 2 * j + h
@@ -1032,31 +1033,21 @@
             along(j, 0).wait_send()
             along_far(j, 0).wait_send()
 
-        for h in range(2):
-            beside(j, h).wait_send()
-            beside_far(j, h).wait_send()
-            for source in range(2):
-                over(j, h, source).wait_send()
-                pair_own(j, h, source).wait_send()
-                pair_far(j, h, source).wait_send()
-
     cross().wait_send()
 
-    @pl.loop(0, units)
-    def _(u):
-        part_near(u).wait_send()
-        part_far(u).wait_send()
-        sum_over(u).wait_send()
-
+    def sent(ref, sem):
+        remote(ref, ref, sem, rgot.at[z], (s, mate)).wait_send()
+
+    sent(ysend, ysem.at[0])
+    sent(far_ysend, fysem.at[0])
+    sent(recv.at[:, :, t, :, :, last_columns], dsend.at[0])
+    sent(recv.at[:, :, t], dsend.at[1])
+    sent(recv.at[:, :, across], dsend.at[2])
+    sent(part.at[:, mate], psend.at[0])
+    sent(part.at[:, mate_across], psend.at[1])
+    sent(psum, psend.at[2])
     gather(z, finish)
-
-    @pl.loop(0, units)
-    def _(u):
-        homeward(u // 2, u % 2, other_y).wait_send()
-
-        @pl.when(u > 1)
-        def _():
-            homeward(u // 2, u % 2, y).wait_send()
+    sent(fin.at[pl.ds(0, units - 1)], hsend.at[0])
 
 
 def relay_body(
@@ -1070,7 +1061,7 @@
     units_hidden = expert_gate.shape[2]
     planes, half = n // 2, cap // 2
     units = 2 * planes
-    halo, pieces = 16, 4
+    halo, pieces = 16, 8
     early = width // 1024 * 384
     part_width = width // pieces
     vmem = pl.BlockSpec(memory_space=pltpu.VMEM)
@@ -1122,20 +1113,20 @@
             dma((planes,)),
             dma((2, planes)),
             dma((planes,)),
+            dma((1,)),
             dma((planes, 2)),
-            dma((planes, 2)),
+            dma((3,)),
             dma((3, planes, 2, 2)),
-            dma((3, planes, 2, 2)),
+            dma((3,)),
             dma((3, units)),
-            dma((3, units)),
-            dma((units, 2)),
+            dma((1,)),
             dma((n, 2)),
             dma((1,)),
             dma((planes,)),
             dma((planes,)),
             dma((2, planes)),
             dma((planes,)),
-            dma((planes, 2)),
+            dma((1,)),
             dma((planes, 2)),
         ],
         compiler_params=pltpu.CompilerParams(

time: 121 us -> 118 us (0.975)
  Pallas kernels: 118 us -> 116 us
    pallas_call x1, Pallas kernels: 118 us -> 116 us  [relay_body(): pl.pallas_call(functools.partial(layer_kernel, n, tp, halo, pieces, cap,...]
where the time goes in v3:
time: 118 us
  Pallas kernels  116 us (98%)
  local copies, waits for them, and re-layouts  1.88 us (2%)
    pallas_call x1, Pallas kernels, relay_body(): pl.pallas_call(functools.partial(layer_kernel, n, tp, halo, pieces, cap,...  116 us

profile of v3, /device:TPU:0, one launch (start us, length us, event | category | flops | bytes accessed | tf_op | source)
XLA Modules:
  0.0 117.6 jit_solution(8120299878599495001)
XLA Ops:
  0.0 115.7 %shard_map.118 = bf16[128,2048]{1,0:T(8,128)(2,1)} custom-call(s32[2,512]{1,0:T(2,128)} %bitcast.10, f32[2,512]{1,0:T(2,128)} %bitcast.11, f32[3,512]{1,0:T(4,128)} %taps_ref.1, f32[1,2048]{1,0:T(1,128)} %bitcast.9, bf16[512,512]{1,0:T(8,128)(2,1)} %gate_hbm.1, bf16[512,512]{1,0:T(8,128)(2,1)} %value_hbm.1, bf16[512,512]{1,0:T(8,128)(2,1)} %out_gate_hbm.1, ...), custom_call_target="tpu_custom_call" | custom-call | tf_op jit(solution)/shard_map/pallas_call | solution.py:1072
  115.7 1.9 %copy.14 = bf16[128,2048]{1,0:T(8,128)(2,1)} copy(bf16[128,2048]{1,0:T(8,128)(2,1)} %shard_map.118) | data formatting | bytes 1048576

commit v4 on v3

--- a/solution.py
+++ b/solution.py
@@ -714,7 +714,7 @@
         ref = recv.at[j, h, across, source]
         return remote(ref, ref, dsend.at[2], dgot.at[2, j, h, source], (s, mate))
 
-    wide = min(512, width)
+    wide = min(1024, width)
 
     def select(raw, info, block, expert, put):
         place = lax.broadcasted_iota(jnp.int32, (cap, quarter), 0).astype(f32) + (

time: 118 us -> 117 us (level)
  no operation moved by 1% of the time
where the time goes in v4:
time: 117 us
  Pallas kernels  115 us (98%)
  local copies, waits for them, and re-layouts  1.88 us (2%)
    pallas_call x1, Pallas kernels, relay_body(): pl.pallas_call(functools.partial(layer_kernel, n, tp, halo, pieces, cap,...  115 us

profile of v4, /device:TPU:0, one launch (start us, length us, event | category | flops | bytes accessed | tf_op | source)
XLA Modules:
  0.0 116.6 jit_solution(13587608447732335777)
XLA Ops:
  0.0 114.7 %shard_map.118 = bf16[128,2048]{1,0:T(8,128)(2,1)} custom-call(s32[2,512]{1,0:T(2,128)} %bitcast.10, f32[2,512]{1,0:T(2,128)} %bitcast.11, f32[3,512]{1,0:T(4,128)} %taps_ref.1, f32[1,2048]{1,0:T(1,128)} %bitcast.9, bf16[512,512]{1,0:T(8,128)(2,1)} %gate_hbm.1, bf16[512,512]{1,0:T(8,128)(2,1)} %value_hbm.1, bf16[512,512]{1,0:T(8,128)(2,1)} %out_gate_hbm.1, ...), custom_call_target="tpu_custom_call" | custom-call | tf_op jit(solution)/shard_map/pallas_call | solution.py:1072
  114.7 1.9 %copy.14 = bf16[128,2048]{1,0:T(8,128)(2,1)} copy(bf16[128,2048]{1,0:T(8,128)(2,1)} %shard_map.118) | data formatting | bytes 1048576
